TPU v7x, 256 devices: a whole 4x4x8 slice. The times are simulated.
256 devices in a mesh: sp: 16 (over y, x), tp: 16 (over z, core).
Axes of the slice: x: 4, y: 4, z: 8, core: 2. Of those that a mesh axis runs over, the one named last changes fastest.
Arguments:
- saved_input: bfloat16 [4096, 2048], P('sp'), may hold values from -6 to 6
- cotangent: bfloat16 [4096, 2048], P('sp'), may hold values from -6 to 6
- expert_ids: int32 [4096, 2], P('sp'), may hold values from 0 to 15, all different within a row; in each aligned block of 256 rows (0 to 255, 256 to 511, ...) at most 64 rows name the same one
- route_weight: float32 [4096, 2], P('sp'), may hold values from 0.1 to 0.9
- w_gate: bfloat16 [16, 2048, 6144], P('sp', None, 'tp'), may hold values from -0.125 to 0.125
- w_up: bfloat16 [16, 2048, 6144], P('sp', None, 'tp'), may hold values from -0.125 to 0.125
- w_down: bfloat16 [16, 6144, 2048], P('sp', 'tp'), may hold values from -0.078125 to 0.078125
- w_out: bfloat16 [2048, 2048], P(None, 'tp'), may hold values from -0.125 to 0.125
- channel_gain: float32 [2048], P('tp'), may hold values from 0.1 to 1.9
- conv_taps: float32 [31, 2048], P(None, 'tp'), may hold values from -1 to 1
- glu_value: bfloat16 [2048, 4096], P('tp', 'sp'), may hold values from -6 to 6
- glu_gate: bfloat16 [2048, 4096], P('tp', 'sp'), may hold values from -8 to 8
- conv_out: bfloat16 [2048, 4096], P('tp', 'sp'), may hold values from -6 to 6
- norm_mean: float32 [4096], P('sp'), may hold values from -3 to 3
- norm_rstd: float32 [4096], P('sp'), may hold values from 0.5 to 2
Outputs:
- gate_grad: bfloat16 [16, 2048, 6144], P('sp', None, 'tp')
- up_grad: bfloat16 [16, 2048, 6144], P('sp', None, 'tp')
- down_grad: bfloat16 [16, 6144, 2048], P('sp', 'tp')
- proj_grad: float32 [2048, 2048], P('sp', 'tp')
- value_grad: bfloat16 [2048, 4096], P('tp', 'sp')
- gate_in_grad: bfloat16 [2048, 4096], P('tp', 'sp')
Inputs may be any that keep to these rules, and one draw needn't show every extreme that they name: `expert_ids`: the two experts of a position differ. In the positions of one block of 256, no expert is named more than 64 times, a bound that some block reaches.
All inputs are finite; a program needn't handle non-finite values.
Results may differ from a plain program's by a relative error of at most 0.018.
Values may be sent and summed in bfloat16 or wider, within the bound.
No kernel may reach another device: no remote copies, remote signals or barrier semaphores. Data moves between devices by JAX's collectives and lax.ppermute only.
A program may use at most 128 MiB of HBM per device.

v0:
```python
import jax
import jax.numpy as jnp
from jax import lax
from jax.sharding import PartitionSpec as P

D = 2048
C = 2048


def in_one_piece(arrays, axis, split_dim, concat_dim, along):
    ends, at = ([], 0)
    for a in arrays[:-1]:
        at += a.shape[along]
        ends.append(at)
    both = jnp.concatenate(arrays, axis=along)
    return tuple(
        jnp.split(
            lax.all_to_all(both, axis, split_axis=split_dim, concat_axis=concat_dim, tiled=True),
            ends,
            axis=along,
        )
    )


def cut_along(value, dim, devices):
    before, after = (value.shape[:dim], value.shape[dim + 1 :])
    return jnp.moveaxis(value.reshape(*before, devices, -1, *after), dim, 0)


def sent_and_summed(value, axis, dim):
    devices = lax.axis_size(axis)
    tiles = lax.all_to_all(cut_along(value, dim, devices), axis, 0, 0, tiled=True)
    return jnp.sum(tiles.astype(jnp.float32), axis=0)


def copy_for_each(value, axis):
    copies = jnp.broadcast_to(value, (lax.axis_size(axis), *value.shape))
    return lax.all_to_all(copies, axis, split_axis=0, concat_axis=0, tiled=True)


def of_everyone(value, axis):
    everything = copy_for_each(value, axis)
    return jnp.sum(everything, axis=0)


def in_one(arrays, axis):
    ravelled, at, gathered = (jnp.concatenate([a.reshape(-1) for a in arrays]), 0, [])
    subtotal = of_everyone(ravelled, axis)
    for a in arrays:
        gathered.append(subtotal[at : at + a.size].reshape(a.shape))
        at += a.size
    return tuple(gathered)


def from_behind(value, axis, by):
    devices = lax.axis_size(axis)
    pairs = [(i, i + by) for i in range(devices) if 0 <= i + by < devices]
    return lax.ppermute(value, axis, pairs)


def contract(left, right, left_dim, right_dim):
    return lax.dot_general(
        left, right, (((left_dim,), (right_dim,)), ((), ())), preferred_element_type=jnp.float32
    )


def expert_grads(rows_in, rows_cot, gate_weight, up_weight, down_weight):
    gate_pre = jnp.dot(rows_in, gate_weight, preferred_element_type=jnp.float32)
    up_pre = jnp.dot(rows_in, up_weight, preferred_element_type=jnp.float32)
    sigma = jax.nn.sigmoid(gate_pre)
    hidden = (gate_pre * sigma * up_pre).astype(jnp.bfloat16)
    hidden_cot = contract(rows_cot, down_weight, 1, 1)
    down_part = contract(hidden, rows_cot, 0, 0).astype(jnp.bfloat16)
    gate_cot = (hidden_cot * up_pre * sigma * (1.0 + gate_pre * (1.0 - sigma))).astype(jnp.bfloat16)
    up_cot = (hidden_cot * gate_pre * sigma).astype(jnp.bfloat16)
    gate_part = contract(rows_in, gate_cot, 0, 0).astype(jnp.bfloat16)
    up_part = contract(rows_in, up_cot, 0, 0).astype(jnp.bfloat16)
    input_cot = contract(gate_cot, gate_weight, 1, 1) + contract(up_cot, up_weight, 1, 1)
    return (gate_part, up_part, down_part, input_cot)


def on_device(
    saved_input,
    cotangent,
    expert_ids,
    route_weight,
    w_gate,
    w_up,
    w_down,
    w_out,
    channel_gain,
    conv_taps,
    glu_value,
    glu_gate,
    conv_out,
    norm_mean,
    norm_rstd,
):
    tokens_here = cotangent.shape[0]
    sp_count = lax.axis_size("sp")
    local_experts = w_gate.shape[0]
    expert_count = local_experts * sp_count
    capacity = 4 * tokens_here // expert_count
    pairs = expert_ids.reshape(2 * tokens_here)
    onehot = (pairs[:, None] == jnp.arange(expert_count, dtype=jnp.int32)[None, :]).astype(
        jnp.int32
    )
    before = jnp.cumsum(onehot, axis=0) - onehot
    target = pairs * capacity + jnp.sum(before * onehot, axis=1)
    owner = (
        jnp.zeros((expert_count * capacity,), jnp.int32)
        .at[target]
        .set(jnp.arange(2 * tokens_here, dtype=jnp.int32) + 1)
    )
    filled = (owner > 0)[:, None]
    pair_index = jnp.maximum(owner - 1, 0)
    scaled = (route_weight[:, :, None] * cotangent.astype(jnp.float32)[:, None, :]).astype(
        jnp.bfloat16
    )
    scaled = scaled.reshape(2 * tokens_here, D)
    send_cot = jnp.where(filled, scaled[pair_index], jnp.zeros_like(scaled[:1])).reshape(
        expert_count, capacity, D
    )
    send_in = jnp.where(filled, saved_input[pair_index // 2], jnp.zeros_like(saved_input[:1]))
    send_in = send_in.reshape(expert_count, capacity, D)
    rows_cot, rows_in = in_one_piece((send_cot, send_in), "sp", 0, 1, 2)
    results = [expert_grads(rows_in[0], rows_cot[0], w_gate[0], w_up[0], w_down[0])]
    gate_grad = jnp.stack([result[0] for result in results])
    up_grad = jnp.stack([result[1] for result in results])
    down_grad = jnp.stack([result[2] for result in results])
    input_cot = jnp.stack([result[3] for result in results])
    blocks = input_cot.reshape(local_experts, sp_count, capacity, D)
    share = lax.psum_scatter(
        blocks.astype(jnp.bfloat16), "tp", scatter_dimension=2, tiled=True
    ).astype(jnp.float32)
    returned = lax.all_to_all(
        share.astype(jnp.bfloat16), "sp", split_axis=1, concat_axis=0, tiled=True
    ).astype(share.dtype)
    whole = lax.all_gather(returned.astype(jnp.bfloat16), "tp", axis=2, tiled=True).astype(
        returned.dtype
    )
    routed = whole.reshape(expert_count * capacity, D)[target].reshape(tokens_here, 2, D)
    summed = jnp.sum(routed, axis=1)
    mixed_cot = (cotangent.astype(jnp.float32) + summed).astype(jnp.bfloat16)
    centered = (conv_out.astype(jnp.float32) - norm_mean[None, :]) * norm_rstd[None, :]
    normed = centered * channel_gain[:, None]
    sigma = jax.nn.sigmoid(normed)
    output_act = (normed * sigma).astype(jnp.bfloat16)
    proj_grad = sent_and_summed(contract(mixed_cot, output_act, 0, 1).astype(jnp.bfloat16), "sp", 0)
    act_cot = contract(w_out, mixed_cot, 0, 1)
    norm_cot = act_cot * sigma * (1.0 + normed * (1.0 - sigma)) * channel_gain[:, None]
    first_sum, second_sum = in_one(
        (jnp.sum(norm_cot, axis=0), jnp.sum(norm_cot * centered, axis=0)), "tp"
    )
    conv_cot = norm_rstd[None, :] * (
        norm_cot - first_sum[None, :] / C - centered * second_sum[None, :] / C
    )
    reach = conv_taps.shape[0] - 1
    rim = from_behind(conv_cot[:, :reach], "sp", -1)
    padded = jnp.concatenate([conv_cot, rim], axis=1)
    glu_cot = conv_taps[0][:, None] * padded[:, :tokens_here]
    for lag in range(1, reach + 1):
        glu_cot = glu_cot + conv_taps[lag][:, None] * padded[:, lag : lag + tokens_here]
    gate_sigma = jax.nn.sigmoid(glu_gate.astype(jnp.float32))
    value_grad = (glu_cot * gate_sigma).astype(jnp.bfloat16)
    gate_in_grad = (
        glu_cot * glu_value.astype(jnp.float32) * gate_sigma * (1.0 - gate_sigma)
    ).astype(jnp.bfloat16)
    return (gate_grad, up_grad, down_grad, proj_grad, value_grad, gate_in_grad)


def solution(mesh):
    in_specs = (
        P("sp", None),
        P("sp", None),
        P("sp", None),
        P("sp", None),
        P("sp", None, "tp"),
        P("sp", None, "tp"),
        P("sp", "tp", None),
        P(None, "tp"),
        P("tp"),
        P(None, "tp"),
        P("tp", "sp"),
        P("tp", "sp"),
        P("tp", "sp"),
        P("sp"),
        P("sp"),
    )
    out_specs = (
        P("sp", None, "tp"),
        P("sp", None, "tp"),
        P("sp", "tp", None),
        P("sp", "tp"),
        P("tp", "sp"),
        P("tp", "sp"),
    )
    return jax.shard_map(
        on_device, mesh=mesh, in_specs=in_specs, out_specs=out_specs, check_vma=False
    )
```

profile of v0, /device:TPU:24, one launch (start us, length us, event | category | flops | bytes accessed | tf_op | source)
XLA Modules:
  0.0 370.5 jit_solution(13635867785435302561)
XLA Ops:
  7.2 0.0 copy-start
  7.2 0.0 reduce-scatter.2.cloned.1.call-start
  7.2 0.8 broadcast_multiply_fusion
  8.0 0.8 copy.65
  8.8 0.1 eq.25
  9.0 0.1 eq.29
  9.1 0.1 copy.64
  9.3 0.1 mul.436
  9.4 1.2 reduce-window.6
  10.6 0.2 slice_reduce_fusion
  10.9 0.1 fusion.114
  11.0 2.4 scatter_custom_fusion
  13.5 5.3 %mul.440 = f32[256,2,2048]{2,1,0:T(2,128)} broadcast(bf16[256,2048]{1,0:T(8,128)(2,1)} %param.16), dimensions={0,2} | broadcast | bytes 5242880 | tf_op jit(solution)/shard_map/mul | solution.py:117
  18.8 6.1 %mul.441 = f32[512,2048]{1,0:T(8,128)} reshape(f32[256,2,2048]{2,1,0:T(2,128)} %mul.440) | data formatting | bytes 8388608 | tf_op jit(solution)/shard_map/mul | solution.py:117
  24.9 0.1 copy.68
  25.0 0.1 mul.438
  25.2 0.1 broadcast_in_dim.46
  25.2 3.8 %multiply_convert_fusion = bf16[512,2048]{1,0:T(8,128)(2,1)} fusion(f32[512,2048]{1,0:T(8,128)} %mul.441, f32[512]{0:T(512)S(1)} %mul.438), kind=kLoop, calls=%fused_computation.8 | loop fusion | flops 2097152 | bytes 6293504 | tf_op jit(solution)/shard_map/convert_element_type | solution.py:117
  29.0 10.8 %gather_fusion = bf16[1024,2048]{1,0:T(8,128)(2,1)} fusion(bf16[512,2048]{1,0:T(8,128)(2,1)} %multiply_convert_fusion, s32[1024]{0:T(1024)S(1)} %get-tuple-element.73), kind=kCustom, calls=%fused_computation | custom fusion | bytes 8392704 | tf_op jit(solution)/shard_map/gather | solution.py:121
  39.8 6.0 %gather_fusion.1 = bf16[1024,2048]{1,0:T(8,128)(2,1)} fusion(bf16[256,2048]{1,0:T(8,128)(2,1)S(1)} %copy-done.2, s32[1024]{0:T(1024)S(1)} %get-tuple-element.74), kind=kCustom, calls=%fused_computation.1 | custom fusion | bytes 8392704 | tf_op jit(solution)/shard_map/gather | solution.py:124
  45.8 5.8 %broadcast_select_fusion.1 = (bf16[16,64,2048]{2,1,0:T(8,128)(2,1)}, bf16[16,64,2048]{2,1,0:T(8,128)(2,1)}) fusion(bf16[16,64,2048]{2,1,0:T(8,128)(2,1)} %bitcast.144, pred[16,64]{1,0:T(8,128)(4,1)S(1)} %broadcast_in_dim.46, bf16[16,64,2048]{2,1,0:T(8,128)(2,1)} %bitcast.145), kind=kLoop, calls=%fused_computation.10 | loop fusion | flops 4194304 | bytes 16778240 | tf_op jit(solution)/shard_map/jit(_where)/select_n | solution.py:121
  51.6 7.8 %pad_maximum_fusion = bf16[16,64,4096]{2,1,0:T(8,128)(2,1)} fusion(bf16[16,64,2048]{2,1,0:T(8,128)(2,1)} %get-tuple-element.78, bf16[16,64,2048]{2,1,0:T(8,128)(2,1)} %get-tuple-element.77), kind=kLoop, calls=%fused_computation.4 | loop fusion | flops 16777216 | bytes 16777216 | tf_op jit(solution)/shard_map/concatenate | solution.py:15
  59.4 101.1 %all_to_all.35 = bf16[16,64,4096]{2,1,0:T(8,128)(2,1)S(1)} all-to-all(bf16[16,64,4096]{2,1,0:T(8,128)(2,1)} %pad_maximum_fusion), channel_id=1, replica_groups=mesh['sp'=16,'tp'=16] {'sp'}, dimensions={0} | all-to-all | bytes 16777216 | tf_op jit(solution)/shard_map/all_to_all | solution.py:18
  160.6 2.3 fusion.3
  162.9 0.2 copy-done.5
  163.1 2.3 fusion.4
  165.5 0.2 copy-done.15
  165.7 2.8 multiply_convert_fusion.2
  168.5 2.4 fusion.8
  170.9 2.4 add_convert_fusion
  173.3 4.3 %copy.69 = bf16[1,16,64,2048]{3,1,0,2:T(8,128)(2,1)} copy(bf16[1,16,64,2048]{3,2,1,0:T(8,128)(2,1)S(1)} %bitcast.146) | data formatting | bytes 8388608 | tf_op jit(solution)/shard_map/convert_element_type | solution.py:134
  177.6 0.0 reduce-scatter.2.cloned.1.call-update
  177.6 0.0 all-gather.3.cloned.1.call-start
  177.6 64.5 %reduce-scatter.2.cloned.1.call-done = bf16[1,16,4,2048]{3,1,0,2:T(8,128)(2,1)} async-done(((bf16[1,16,64,2048]{3,1,0,2:T(8,128)(2,1)}), bf16[1,16,4,2048]{3,1,0,2:T(8,128)(2,1)}) %reduce-scatter.2.cloned.1.call-update) | async-done | bytes 262160 | tf_op jit(solution)/shard_map/reduce_scatter | solution.py:133
  242.2 1.2 copy.70
  243.3 13.6 %all_to_all.36 = bf16[1,16,4,2048]{3,2,0,1:T(4,128)(2,1)S(1)} all-to-all(bf16[1,16,4,2048]{3,2,0,1:T(4,128)(2,1)S(1)} %copy.70), channel_id=1, replica_groups=mesh['sp'=16,'tp'=16] {'sp'}, dimensions={1} | all-to-all | bytes 524288 | tf_op jit(solution)/shard_map/all_to_all | solution.py:136
  256.9 0.9 copy.71
  257.8 0.0 all-gather.3.cloned.1.call-update
  257.8 0.1 copy.73
  257.9 0.1 copy.76
  258.1 0.1 copy.75
  258.3 0.0 copy-start.19
  258.3 5.9 %fusion.5 = bf16[1,2048,384]{2,1,0:T(8,128)(2,1)} fusion(bf16[1024,384]{1,0:T(8,128)(2,1)S(1)} %get-tuple-element.41, bf16[1,1024,4096]{2,1,0:T(8,128)(2,1)} %bitcast.150), kind=kOutput, calls=%fused_computation.18 | convolution fusion | flops 1611399168 | bytes 6553600 | tf_op jit(solution)/shard_map/dot_general | solution.py:62
  264.1 5.4 %fusion.7 = bf16[1,384,2048]{2,1,0:T(8,128)(2,1)} fusion(bf16[1,1024,4096]{2,1,0:T(8,128)(2,1)} %bitcast.151, f32[1024,384]{1,0:T(8,128)S(1)} %copy-done.19, f32[1024,384]{1,0:T(8,128)S(1)} %copy-done.17), kind=kOutput, calls=%fused_computation.20 | convolution fusion | flops 1613758464 | bytes 8912896 | tf_op jit(solution)/shard_map/dot_general | solution.py:62
  269.5 26.8 %all-gather.3.cloned.1.call-done = bf16[1,16,64,2048]{3,1,0,2:T(8,128)(2,1)} async-done(((bf16[1,16,4,2048]{3,1,0,2:T(8,128)(2,1)}), bf16[1,16,64,2048]{3,1,0,2:T(8,128)(2,1)}) %all-gather.3.cloned.1.call-update) | async-done | bytes 4194320 | tf_op jit(solution)/shard_map/all_gather | solution.py:139
  296.3 7.8 %copy.72 = f32[1,16,64,2048]{3,2,1,0:T(8,128)} copy(bf16[1,16,64,2048]{3,1,0,2:T(8,128)(2,1)} %all-gather.3.cloned.1.call-done) | data formatting | bytes 12582912 | tf_op jit(solution)/shard_map/reshape | solution.py:142
  304.2 8.8 %gather_fusion.2 = f32[512,2048]{1,0:T(8,128)} fusion(f32[1024,2048]{1,0:T(8,128)} %bitcast.143, s32[1024]{0:T(1024)S(1)} %pad_clamp_fusion), kind=kCustom, calls=%fused_computation.2 | custom fusion | bytes 8390656 | tf_op jit(solution)/shard_map/gather | solution.py:142
  312.9 6.0 %reshape.159 = f32[256,2,2048]{2,1,0:T(2,128)} reshape(f32[512,2048]{1,0:T(8,128)} %gather_fusion.2) | data formatting | bytes 8388608 | tf_op jit(solution)/shard_map/reshape | solution.py:142
  319.0 0.0 copy-start.3
  319.0 0.0 copy-start.6
  319.0 8.6 %reduce_sum.58 = f32[256,2048]{1,0:T(8,128)} reduce(f32[256,2,2048]{2,1,0:T(2,128)} %reshape.159, f32[]{:T(128)} %constant.44.clone.1), dimensions={1}, to_apply=%region_5.6 | reduce | flops 524288 | bytes 6291460 | tf_op jit(solution)/shard_map/reduce_sum | solution.py:143
  327.7 2.1 fusion.123
  329.8 0.6 broadcast_in_dim.51
  330.5 4.4 %all-to-all-start.3 = ((f32[16,1,512]{2,1,0:T(1,128)}), f32[16,1,512]{2,1,0:T(1,128)S(1)}, u32[]{:S(2)}, u32[]{:S(2)}) async-start(f32[16,1,512]{2,1,0:T(1,128)} %broadcast_in_dim.51), calls=%async_computation.4 | async-start | bytes 65536 | tf_op jit(solution)/shard_map/all_to_all | solution.py:38
  334.9 3.1 convolution_convert_fusion.2
  337.9 4.6 %all-to-all-done.3 = f32[16,1,512]{2,1,0:T(1,128)S(1)} async-done(((f32[16,1,512]{2,1,0:T(1,128)}), f32[16,1,512]{2,1,0:T(1,128)S(1)}, u32[]{:S(2)}, u32[]{:S(2)}) %all-to-all-start.3) | async-done | bytes 32800 | tf_op jit(solution)/shard_map/all_to_all | solution.py:38
  342.5 7.2 %all-to-all-start.2 = ((bf16[16,128,128]{2,1,0:T(8,128)(2,1)}), bf16[16,128,128]{2,1,0:T(8,128)(2,1)S(1)}, u32[]{:S(2)}, u32[]{:S(2)}) async-start(bf16[16,128,128]{2,1,0:T(8,128)(2,1)} %bitcast.16), calls=%async_computation.3 | async-start | bytes 1048576 | tf_op jit(solution)/shard_map/all_to_all | solution.py:32
  349.8 0.2 subtract_multiply_fusion
  350.0 4.9 %collective-permute-start = (f32[128,30]{0,1:T(8,128)S(1)}, f32[128,30]{0,1:T(8,128)S(1)}, u32[]{:S(2)}, u32[]{:S(2)}) collective-permute-start(f32[128,30]{0,1:T(8,128)S(1)} %slice.271), channel_id=1, source_target_pairs={{16,0},{32,16},{48,32},{64,48},{80,64},{96,80},{112,96},{128,112},... | collective-permute-start | bytes 46088 | tf_op jit(solution)/shard_map/ppermute | solution.py:58
  354.9 5.8 %fusion.6 = bf16[1,2048,384]{2,1,0:T(8,128)(2,1)} fusion(bf16[1024,384]{1,0:T(8,128)(2,1)S(1)} %get-tuple-element.40, bf16[1,1024,4096]{2,1,0:T(8,128)(2,1)} %bitcast.152), kind=kOutput, calls=%fused_computation.19 | convolution fusion | flops 1611399168 | bytes 6553600 | tf_op jit(solution)/shard_map/dot_general | solution.py:62
  360.8 0.4 multiply_convert_fusion.5
  361.2 0.7 copy.77
  362.0 0.7 copy.78
  362.7 0.7 convert_reduce_fusion
  (51 shorter events, 0.3 us)
Async XLA Ops:
  7.2 153.4 %copy-start = (bf16[1,2048,384]{2,1,0:T(8,128)(2,1)S(1)}, bf16[1,2048,384]{2,1,0:T(8,128)(2,1)}, u32[]{:S(2)}) copy-start(bf16[1,2048,384]{2,1,0:T(8,128)(2,1)} %param.19) | copy-start | bytes 4718596
  7.2 235.0 %reduce-scatter.2.cloned.1.call-start = ((), (), s32[]{:S(2)}) async-start(), calls=%async_computation.5 | async-start | bytes 4456448 | tf_op jit(solution)/shard_map/reduce_scatter | solution.py:133
  18.8 6.1 %copy-start.13 = (f32[256,2]{0,1:T(2,128)S(1)}, f32[256,2]{0,1:T(2,128)}, u32[]{:S(2)}) copy-start(f32[256,2]{0,1:T(2,128)} %param.18) | copy-start | bytes 6148
  29.0 10.8 %copy-start.2 = (bf16[256,2048]{1,0:T(8,128)(2,1)S(1)}, bf16[256,2048]{1,0:T(8,128)(2,1)}, u32[]{:S(2)}) copy-start(bf16[256,2048]{1,0:T(8,128)(2,1)} %param.15) | copy-start | bytes 3145732
  160.6 4.9 %copy-start.4 = (bf16[16,64,4096]{2,1,0:T(8,128)(2,1)}, bf16[16,64,4096]{2,1,0:T(8,128)(2,1)S(1)}, u32[]{:S(2)}) copy-start(bf16[16,64,4096]{2,1,0:T(8,128)(2,1)S(1)} %all_to_all.35) | copy-start | bytes 25165828
  160.6 2.6 copy-start.5
  163.1 2.4 copy-start.16
  163.1 2.6 copy-start.15
  165.7 2.8 copy-start.18
  177.6 80.2 %copy-start.7 = (bf16[128,256]{1,0:T(8,128)(2,1)S(1)}, bf16[128,256]{1,0:T(8,128)(2,1)}, u32[]{:S(2)}) copy-start(bf16[128,256]{1,0:T(8,128)(2,1)} %param.27) | copy-start | bytes 196612
  177.6 80.4 %copy-start.8 = (bf16[128,256]{1,0:T(8,128)(2,1)S(1)}, bf16[128,256]{1,0:T(8,128)(2,1)}, u32[]{:S(2)}) copy-start(bf16[128,256]{1,0:T(8,128)(2,1)} %param.25) | copy-start | bytes 196612
  177.6 80.5 %copy-start.9 = (bf16[128,256]{1,0:T(8,128)(2,1)S(1)}, bf16[128,256]{1,0:T(8,128)(2,1)}, u32[]{:S(2)}) copy-start(bf16[128,256]{1,0:T(8,128)(2,1)} %param.26) | copy-start | bytes 196612
  177.6 80.6 %copy-start.10 = (f32[31,128]{1,0:T(8,128)S(1)}, f32[31,128]{1,0:T(8,128)}, u32[]{:S(2)}) copy-start(f32[31,128]{1,0:T(8,128)} %param.24) | copy-start | bytes 47620
  177.6 118.7 %all-gather.3.cloned.1.call-start = ((), (), s32[]{:S(2)}) async-start(), calls=%async_computation.6 | async-start | bytes 4456448 | tf_op jit(solution)/shard_map/all_gather | solution.py:139
  258.2 5.9 %copy-start.17 = (f32[1024,384]{1,0:T(8,128)S(1)}, f32[1024,384]{1,0:T(8,128)}, u32[]{:S(2)}) copy-start(f32[1024,384]{1,0:T(8,128)} %copy-done.16) | copy-start | bytes 4718596
  258.3 5.9 %copy-start.19 = (f32[1024,384]{1,0:T(8,128)S(1)}, f32[1024,384]{1,0:T(8,128)}, u32[]{:S(2)}) copy-start(f32[1024,384]{1,0:T(8,128)} %copy-done.18) | copy-start | bytes 4718596
  319.0 8.7 %copy-start.3 = (bf16[256,2048]{1,0:T(8,128)(2,1)S(1)}, bf16[256,2048]{1,0:T(8,128)(2,1)}, u32[]{:S(2)}) copy-start(bf16[256,2048]{1,0:T(8,128)(2,1)} %param.16) | copy-start | bytes 3145732
  319.0 8.7 %copy-start.6 = (bf16[2048,128]{1,0:T(8,128)(2,1)S(1)}, bf16[2048,128]{1,0:T(8,128)(2,1)}, u32[]{:S(2)}) copy-start(bf16[2048,128]{1,0:T(8,128)(2,1)} %param.22) | copy-start | bytes 1572868
  319.0 8.7 %copy-start.11 = (f32[256]{0:T(256)S(1)}, f32[256]{0:T(256)}, u32[]{:S(2)}) copy-start(f32[256]{0:T(256)} %param.29) | copy-start | bytes 3076
  319.0 8.7 %copy-start.12 = (f32[256]{0:T(256)S(1)}, f32[256]{0:T(256)}, u32[]{:S(2)}) copy-start(f32[256]{0:T(256)} %param.28) | copy-start | bytes 3076
  319.0 8.7 %copy-start.14 = (f32[128]{0:T(128)S(1)}, f32[128]{0:T(128)}, u32[]{:S(2)}) copy-start(f32[128]{0:T(128)} %param.23) | copy-start | bytes 1540
  330.5 12.1 %all-to-all-start.3 = ((f32[16,1,512]{2,1,0:T(1,128)}), f32[16,1,512]{2,1,0:T(1,128)S(1)}, u32[]{:S(2)}, u32[]{:S(2)}) async-start(f32[16,1,512]{2,1,0:T(1,128)} %broadcast_in_dim.51), calls=%async_computation.4 | async-start | bytes 65536 | tf_op jit(solution)/shard_map/all_to_all | solution.py:38
  342.5 20.2 %all-to-all-start.2 = ((bf16[16,128,128]{2,1,0:T(8,128)(2,1)}), bf16[16,128,128]{2,1,0:T(8,128)(2,1)S(1)}, u32[]{:S(2)}, u32[]{:S(2)}) async-start(bf16[16,128,128]{2,1,0:T(8,128)(2,1)} %bitcast.16), calls=%async_computation.3 | async-start | bytes 1048576 | tf_op jit(solution)/shard_map/all_to_all | solution.py:32
  350.0 10.7 %collective-permute-start = (f32[128,30]{0,1:T(8,128)S(1)}, f32[128,30]{0,1:T(8,128)S(1)}, u32[]{:S(2)}, u32[]{:S(2)}) collective-permute-start(f32[128,30]{0,1:T(8,128)S(1)} %slice.271), channel_id=1, source_target_pairs={{16,0},{32,16},{48,32},{64,48},{80,64},{96,80},{112,96},{128,112},... | collective-permute-start | bytes 46088 | tf_op jit(solution)/shard_map/ppermute | solution.py:58
  354.9 8.5 %copy-start.1 = (bf16[1,2048,384]{2,1,0:T(8,128)(2,1)S(1)}, bf16[1,2048,384]{2,1,0:T(8,128)(2,1)}, u32[]{:S(2)}) copy-start(bf16[1,2048,384]{2,1,0:T(8,128)(2,1)} %param.19) | copy-start | bytes 4718596
Sparse Core Ops, SparseCore 0:
  177.7 64.3 reduce-scatter.1
  257.9 38.3 all-gather.2
where the time goes:
time: 377 us; the launch traced here: 370 us
  blocking collectives  115 us (31%)
  waiting for transfers between devices  95.9 us (25%)
  local copies, waits for them, and re-layouts  64.5 us (17%)
  matrix products  34.5 us (9%)
  other arithmetic  29.5 us (8%)
  starting transfers between devices  16.6 us (4%)
  between operations  14.6 us (4%)
    all_to_all x1, blocking collectives, in_one_piece(): lax.all_to_all(both, axis, split_axis=split_dim, concat_axis=concat_dim,...  101 us
    reduce_scatter x1, waiting for transfers between devices, on_device(): lax.psum_scatter(blocks.astype(jnp.bfloat16), 'tp', scatter_dimension=2,...  64.5 us
    dot_general x8, matrix products, contract(): lax.dot_general(left, right, (((left_dim,), (right_dim,)), ((), ())), pre...  29.9 us
    all_gather x1, waiting for transfers between devices, on_device(): lax.all_gather(returned.astype(jnp.bfloat16), 'tp', axis=2, tiled=True)  26.8 us
    reshape x2, local copies, waits for them, and re-layouts, on_device(): whole.reshape(expert_count * capacity, D)[target].reshape(tokens_here, 2, D)  13.9 us
    all_to_all x1, blocking collectives, on_device(): lax.all_to_all(share.astype(jnp.bfloat16), 'sp', split_axis=1, concat_axi...  13.6 us
    mul x3, local copies, waits for them, and re-layouts, on_device(): route_weight[:, :, None] * cotangent.astype(jnp.float32)[:, None, :]  11.6 us
    gather x1, local copies, waits for them, and re-layouts, on_device(): scaled[pair_index]  10.8 us
  transfers between devices with their start and end apart: 5, of which 3 were waited for; matrix products, arithmetic and copies ran while one was open for 6% of the time, Pallas kernels for 0%

commit v1 on v0

--- a/solution.py
+++ b/solution.py
@@ -136,7 +136,7 @@
     returned = lax.all_to_all(
         share.astype(jnp.bfloat16), "sp", split_axis=1, concat_axis=0, tiled=True
     ).astype(share.dtype)
-    whole = lax.all_gather(returned.astype(jnp.bfloat16), "tp", axis=2, tiled=True).astype(
+    whole = jnp.concatenate(lax.all_gather(returned.astype(jnp.bfloat16), "tp"), axis=2).astype(
         returned.dtype
     )
     routed = whole.reshape(expert_count * capacity, D)[target].reshape(tokens_here, 2, D)

time: 377 us -> 398 us (1.056)
  local copies, waits for them, and re-layouts: 64.5 us -> 78.7 us
  other arithmetic: 29.5 us -> 36 us
    convert_element_type x0 -> x2, local copies, waits for them, and re-layouts: none -> 22 us  [on_device(): jnp.concatenate(lax.all_gather(returned.astype(jnp.bfloat16), 'tp'), axis=2)]
    reshape x2 -> x1, local copies, waits for them, and re-layouts: 13.9 us -> 5.84 us  [on_device(): whole.reshape(expert_count * capacity, D)[target].reshape(tokens_here, 2, D)]
    convert_element_type x0 -> x1, other arithmetic: none -> 6.48 us  [on_device(): jnp.concatenate(lax.all_gather(returned.astype(jnp.bfloat16), 'tp'), axis=2)]
where the time goes in v1:
time: 398 us; the launch traced here: 391 us
  blocking collectives  115 us (29%)
  waiting for transfers between devices  95.9 us (24%)
  local copies, waits for them, and re-layouts  78.7 us (20%)
  other arithmetic  36 us (9%)
  matrix products  34.6 us (9%)
  starting transfers between devices  16.8 us (4%)
  between operations  14.7 us (4%)
    all_to_all x1, blocking collectives, in_one_piece(): lax.all_to_all(both, axis, split_axis=split_dim, concat_axis=concat_dim,...  101 us
    reduce_scatter x1, waiting for transfers between devices, on_device(): lax.psum_scatter(blocks.astype(jnp.bfloat16), 'tp', scatter_dimension=2,...  64.5 us
    dot_general x8, matrix products, contract(): lax.dot_general(left, right, (((left_dim,), (right_dim,)), ((), ())), pre...  29.9 us
    all_gather x1, waiting for transfers between devices, on_device(): lax.all_gather(returned.astype(jnp.bfloat16), 'tp')  26.8 us
    convert_element_type x2, local copies, waits for them, and re-layouts, on_device(): jnp.concatenate(lax.all_gather(returned.astype(jnp.bfloat16), 'tp'), axis=2)  22 us
    all_to_all x1, blocking collectives, on_device(): lax.all_to_all(share.astype(jnp.bfloat16), 'sp', split_axis=1, concat_axi...  13.6 us
    mul x3, local copies, waits for them, and re-layouts, on_device(): route_weight[:, :, None] * cotangent.astype(jnp.float32)[:, None, :]  11.6 us
    gather x1, local copies, waits for them, and re-layouts, on_device(): scaled[pair_index]  10.8 us
  transfers between devices with their start and end apart: 5, of which 3 were waited for; matrix products, arithmetic and copies ran while one was open for 6% of the time, Pallas kernels for 0%

profile of v1, /device:TPU:24, one launch (start us, length us, event | category | flops | bytes accessed | tf_op | source)
XLA Modules:
  0.0 391.4 jit_solution(15545123315410769565)
XLA Ops:
  7.2 0.0 copy-start
  7.2 0.0 reduce-scatter.2.cloned.1.call-start
  7.2 0.8 broadcast_multiply_fusion
  8.0 0.8 copy.67
  8.8 0.1 eq.25
  9.0 0.1 eq.29
  9.1 0.1 copy.66
  9.3 0.1 mul.436
  9.4 1.2 reduce-window.6
  10.6 0.2 slice_reduce_fusion
  10.9 0.1 fusion.114
  11.0 2.4 scatter_custom_fusion
  13.5 5.3 %mul.440 = f32[256,2,2048]{2,1,0:T(2,128)} broadcast(bf16[256,2048]{1,0:T(8,128)(2,1)} %param.16), dimensions={0,2} | broadcast | bytes 5242880 | tf_op jit(solution)/shard_map/mul | solution.py:117
  18.8 6.1 %mul.441 = f32[512,2048]{1,0:T(8,128)} reshape(f32[256,2,2048]{2,1,0:T(2,128)} %mul.440) | data formatting | bytes 8388608 | tf_op jit(solution)/shard_map/mul | solution.py:117
  24.9 0.1 copy.70
  25.0 0.1 mul.438
  25.2 0.1 broadcast_in_dim.46
  25.2 3.8 multiply_convert_fusion
  29.0 10.8 %gather_fusion = bf16[1024,2048]{1,0:T(8,128)(2,1)} fusion(bf16[512,2048]{1,0:T(8,128)(2,1)} %multiply_convert_fusion, s32[1024]{0:T(1024)S(1)} %get-tuple-element.73), kind=kCustom, calls=%fused_computation | custom fusion | bytes 8392704 | tf_op jit(solution)/shard_map/gather | solution.py:121
  39.8 6.0 %gather_fusion.1 = bf16[1024,2048]{1,0:T(8,128)(2,1)} fusion(bf16[256,2048]{1,0:T(8,128)(2,1)S(1)} %copy-done.2, s32[1024]{0:T(1024)S(1)} %get-tuple-element.74), kind=kCustom, calls=%fused_computation.1 | custom fusion | bytes 8392704 | tf_op jit(solution)/shard_map/gather | solution.py:124
  45.8 5.8 %broadcast_select_fusion.1 = (bf16[16,64,2048]{2,1,0:T(8,128)(2,1)}, bf16[16,64,2048]{2,1,0:T(8,128)(2,1)}) fusion(bf16[16,64,2048]{2,1,0:T(8,128)(2,1)} %bitcast.149, pred[16,64]{1,0:T(8,128)(4,1)S(1)} %broadcast_in_dim.46, bf16[16,64,2048]{2,1,0:T(8,128)(2,1)} %bitcast.150), kind=kLoop, calls=%fused_computation.11 | loop fusion | flops 4194304 | bytes 16778240 | tf_op jit(solution)/shard_map/jit(_where)/select_n | solution.py:121
  51.6 7.8 %pad_maximum_fusion = bf16[16,64,4096]{2,1,0:T(8,128)(2,1)} fusion(bf16[16,64,2048]{2,1,0:T(8,128)(2,1)} %get-tuple-element.78, bf16[16,64,2048]{2,1,0:T(8,128)(2,1)} %get-tuple-element.77), kind=kLoop, calls=%fused_computation.4 | loop fusion | flops 16777216 | bytes 16777216 | tf_op jit(solution)/shard_map/concatenate | solution.py:15
  59.4 101.2 %all_to_all.35 = bf16[16,64,4096]{2,1,0:T(8,128)(2,1)S(1)} all-to-all(bf16[16,64,4096]{2,1,0:T(8,128)(2,1)} %pad_maximum_fusion), channel_id=1, replica_groups=mesh['sp'=16,'tp'=16] {'sp'}, dimensions={0} | all-to-all | bytes 16777216 | tf_op jit(solution)/shard_map/all_to_all | solution.py:18
  160.6 2.3 fusion.3
  163.0 0.2 copy-done.5
  163.2 2.3 fusion.4
  165.6 0.2 copy-done.15
  165.8 2.8 multiply_convert_fusion.2
  168.6 2.4 fusion.8
  170.9 2.4 add_convert_fusion
  173.4 4.3 %copy.71 = bf16[1,16,64,2048]{3,1,0,2:T(8,128)(2,1)} copy(bf16[1,16,64,2048]{3,2,1,0:T(8,128)(2,1)S(1)} %bitcast.151) | data formatting | bytes 8388608 | tf_op jit(solution)/shard_map/convert_element_type | solution.py:134
  177.6 0.0 reduce-scatter.2.cloned.1.call-update
  177.7 0.0 all-gather.3.cloned.1.call-start
  177.7 64.5 %reduce-scatter.2.cloned.1.call-done = bf16[1,16,4,2048]{3,1,0,2:T(8,128)(2,1)} async-done(((bf16[1,16,64,2048]{3,1,0,2:T(8,128)(2,1)}), bf16[1,16,4,2048]{3,1,0,2:T(8,128)(2,1)}) %reduce-scatter.2.cloned.1.call-update) | async-done | bytes 262160 | tf_op jit(solution)/shard_map/reduce_scatter | solution.py:133
  242.2 1.2 copy.72
  243.4 13.6 %all_to_all.36 = bf16[1,16,4,2048]{3,2,0,1:T(4,128)(2,1)S(1)} all-to-all(bf16[1,16,4,2048]{3,2,0,1:T(4,128)(2,1)S(1)} %copy.72), channel_id=1, replica_groups=mesh['sp'=16,'tp'=16] {'sp'}, dimensions={1} | all-to-all | bytes 524288 | tf_op jit(solution)/shard_map/all_to_all | solution.py:136
  257.0 0.9 copy.73
  257.8 0.0 all-gather.3.cloned.1.call-update
  257.9 0.1 copy.75
  258.0 0.1 copy.78
  258.1 0.1 copy.77
  258.3 0.0 copy-start.19
  258.3 5.9 %fusion.5 = bf16[1,2048,384]{2,1,0:T(8,128)(2,1)} fusion(bf16[1024,384]{1,0:T(8,128)(2,1)S(1)} %get-tuple-element.41, bf16[1,1024,4096]{2,1,0:T(8,128)(2,1)} %bitcast.155), kind=kOutput, calls=%fused_computation.19 | convolution fusion | flops 1611399168 | bytes 6553600 | tf_op jit(solution)/shard_map/dot_general | solution.py:62
  264.2 5.4 %fusion.7 = bf16[1,384,2048]{2,1,0:T(8,128)(2,1)} fusion(bf16[1,1024,4096]{2,1,0:T(8,128)(2,1)} %bitcast.156, f32[1024,384]{1,0:T(8,128)S(1)} %copy-done.19, f32[1024,384]{1,0:T(8,128)S(1)} %copy-done.17), kind=kOutput, calls=%fused_computation.21 | convolution fusion | flops 1613758464 | bytes 8912896 | tf_op jit(solution)/shard_map/dot_general | solution.py:62
  269.6 26.8 %all-gather.3.cloned.1.call-done = bf16[16,16,4,2048]{3,1,2,0:T(8,128)(2,1)} async-done(((bf16[1,16,4,2048]{3,1,2,0:T(8,128)(2,1)}), bf16[16,16,4,2048]{3,1,2,0:T(8,128)(2,1)}) %all-gather.3.cloned.1.call-update) | async-done | bytes 4194320 | tf_op jit(solution)/shard_map/all_gather | solution.py:139
  296.4 6.5 %convert_bitcast_fusion = f32[16,1,16,4,2048]{4,0,3,2,1:T(8,128)} fusion(bf16[16,16,4,2048]{3,1,2,0:T(8,128)(2,1)} %all-gather.3.cloned.1.call-done), kind=kLoop, calls=%fused_computation.5 | loop fusion | flops 2097152 | bytes 12582912 | tf_op jit(solution)/shard_map/convert_element_type | solution.py:139
  302.9 12.0 %copy.74 = f32[16,1,16,4,2048]{4,3,2,0,1:T(4,128)} copy(f32[16,1,16,4,2048]{4,0,3,2,1:T(8,128)} %convert_bitcast_fusion) | data formatting | bytes 16777216 | tf_op jit(solution)/shard_map/convert_element_type | solution.py:139
  314.9 10.0 %reshape.162 = f32[1024,2048]{1,0:T(8,128)} reshape(f32[16,1,16,4,2048]{4,3,2,0,1:T(4,128)} %copy.74) | data formatting | bytes 16777216 | tf_op jit(solution)/shard_map/convert_element_type | solution.py:139
  324.9 9.0 %gather_fusion.2 = f32[512,2048]{1,0:T(8,128)} fusion(f32[1024,2048]{1,0:T(8,128)} %reshape.162, s32[1024]{0:T(1024)S(1)} %pad_clamp_fusion), kind=kCustom, calls=%fused_computation.2 | custom fusion | bytes 8390656 | tf_op jit(solution)/shard_map/gather | solution.py:142
  333.8 5.8 %reshape.160 = f32[256,2,2048]{2,1,0:T(2,128)} reshape(f32[512,2048]{1,0:T(8,128)} %gather_fusion.2) | data formatting | bytes 8388608 | tf_op jit(solution)/shard_map/reshape | solution.py:142
  339.7 8.6 %reduce_sum.58 = f32[256,2048]{1,0:T(8,128)} reduce(f32[256,2,2048]{2,1,0:T(2,128)} %reshape.160, f32[]{:T(128)} %constant.44.clone.1), dimensions={1}, to_apply=%region_5.6 | reduce | flops 524288 | bytes 6291460 | tf_op jit(solution)/shard_map/reduce_sum | solution.py:143
  348.3 2.1 fusion.123
  350.5 0.6 broadcast_in_dim.51
  351.1 4.4 %all-to-all-start.3 = ((f32[16,1,512]{2,1,0:T(1,128)}), f32[16,1,512]{2,1,0:T(1,128)S(1)}, u32[]{:S(2)}, u32[]{:S(2)}) async-start(f32[16,1,512]{2,1,0:T(1,128)} %broadcast_in_dim.51), calls=%async_computation.4 | async-start | bytes 65536 | tf_op jit(solution)/shard_map/all_to_all | solution.py:38
  355.5 3.1 convolution_convert_fusion.2
  358.6 4.6 %all-to-all-done.3 = f32[16,1,512]{2,1,0:T(1,128)S(1)} async-done(((f32[16,1,512]{2,1,0:T(1,128)}), f32[16,1,512]{2,1,0:T(1,128)S(1)}, u32[]{:S(2)}, u32[]{:S(2)}) %all-to-all-start.3) | async-done | bytes 32800 | tf_op jit(solution)/shard_map/all_to_all | solution.py:38
  363.2 7.2 %all-to-all-start.2 = ((bf16[16,128,128]{2,1,0:T(8,128)(2,1)}), bf16[16,128,128]{2,1,0:T(8,128)(2,1)S(1)}, u32[]{:S(2)}, u32[]{:S(2)}) async-start(bf16[16,128,128]{2,1,0:T(8,128)(2,1)} %bitcast.17), calls=%async_computation.3 | async-start | bytes 1048576 | tf_op jit(solution)/shard_map/all_to_all | solution.py:32
  370.5 0.2 subtract_multiply_fusion
  370.7 5.1 %collective-permute-start = (f32[128,30]{0,1:T(8,128)S(1)}, f32[128,30]{0,1:T(8,128)S(1)}, u32[]{:S(2)}, u32[]{:S(2)}) collective-permute-start(f32[128,30]{0,1:T(8,128)S(1)} %slice.271), channel_id=1, source_target_pairs={{16,0},{32,16},{48,32},{64,48},{80,64},{96,80},{112,96},{128,112},... | collective-permute-start | bytes 46088 | tf_op jit(solution)/shard_map/ppermute | solution.py:58
  375.8 5.8 %fusion.6 = bf16[1,2048,384]{2,1,0:T(8,128)(2,1)} fusion(bf16[1024,384]{1,0:T(8,128)(2,1)S(1)} %get-tuple-element.40, bf16[1,1024,4096]{2,1,0:T(8,128)(2,1)} %bitcast.157), kind=kOutput, calls=%fused_computation.20 | convolution fusion | flops 1611399168 | bytes 6553600 | tf_op jit(solution)/shard_map/dot_general | solution.py:62
  381.7 0.4 multiply_convert_fusion.5
  382.1 0.7 copy.79
  382.9 0.7 copy.80
  383.6 0.7 convert_reduce_fusion
  (53 shorter events, 0.3 us)
Async XLA Ops:
  7.2 153.5 %copy-start = (bf16[1,2048,384]{2,1,0:T(8,128)(2,1)S(1)}, bf16[1,2048,384]{2,1,0:T(8,128)(2,1)}, u32[]{:S(2)}) copy-start(bf16[1,2048,384]{2,1,0:T(8,128)(2,1)} %param.19) | copy-start | bytes 4718596
  7.2 235.0 %reduce-scatter.2.cloned.1.call-start = ((), (), s32[]{:S(2)}) async-start(), calls=%async_computation.5 | async-start | bytes 4456448 | tf_op jit(solution)/shard_map/reduce_scatter | solution.py:133
  18.8 6.1 %copy-start.13 = (f32[256,2]{0,1:T(2,128)S(1)}, f32[256,2]{0,1:T(2,128)}, u32[]{:S(2)}) copy-start(f32[256,2]{0,1:T(2,128)} %param.18) | copy-start | bytes 6148
  29.0 10.8 %copy-start.2 = (bf16[256,2048]{1,0:T(8,128)(2,1)S(1)}, bf16[256,2048]{1,0:T(8,128)(2,1)}, u32[]{:S(2)}) copy-start(bf16[256,2048]{1,0:T(8,128)(2,1)} %param.15) | copy-start | bytes 3145732
  160.6 4.9 %copy-start.4 = (bf16[16,64,4096]{2,1,0:T(8,128)(2,1)}, bf16[16,64,4096]{2,1,0:T(8,128)(2,1)S(1)}, u32[]{:S(2)}) copy-start(bf16[16,64,4096]{2,1,0:T(8,128)(2,1)S(1)} %all_to_all.35) | copy-start | bytes 25165828
  160.6 2.6 copy-start.5
  163.2 2.4 copy-start.16
  163.2 2.6 copy-start.15
  165.8 2.8 copy-start.18
  177.6 80.2 %copy-start.7 = (bf16[128,256]{1,0:T(8,128)(2,1)S(1)}, bf16[128,256]{1,0:T(8,128)(2,1)}, u32[]{:S(2)}) copy-start(bf16[128,256]{1,0:T(8,128)(2,1)} %param.27) | copy-start | bytes 196612
  177.6 80.4 %copy-start.8 = (bf16[128,256]{1,0:T(8,128)(2,1)S(1)}, bf16[128,256]{1,0:T(8,128)(2,1)}, u32[]{:S(2)}) copy-start(bf16[128,256]{1,0:T(8,128)(2,1)} %param.25) | copy-start | bytes 196612
  177.6 80.5 %copy-start.9 = (bf16[128,256]{1,0:T(8,128)(2,1)S(1)}, bf16[128,256]{1,0:T(8,128)(2,1)}, u32[]{:S(2)}) copy-start(bf16[128,256]{1,0:T(8,128)(2,1)} %param.26) | copy-start | bytes 196612
  177.6 80.6 %copy-start.10 = (f32[31,128]{1,0:T(8,128)S(1)}, f32[31,128]{1,0:T(8,128)}, u32[]{:S(2)}) copy-start(f32[31,128]{1,0:T(8,128)} %param.24) | copy-start | bytes 47620
  177.7 118.7 %all-gather.3.cloned.1.call-start = ((), (), s32[]{:S(2)}) async-start(), calls=%async_computation.6 | async-start | bytes 4456448 | tf_op jit(solution)/shard_map/all_gather | solution.py:139
  258.3 5.9 %copy-start.17 = (f32[1024,384]{1,0:T(8,128)S(1)}, f32[1024,384]{1,0:T(8,128)}, u32[]{:S(2)}) copy-start(f32[1024,384]{1,0:T(8,128)} %copy-done.16) | copy-start | bytes 4718596
  258.3 5.9 %copy-start.19 = (f32[1024,384]{1,0:T(8,128)S(1)}, f32[1024,384]{1,0:T(8,128)}, u32[]{:S(2)}) copy-start(f32[1024,384]{1,0:T(8,128)} %copy-done.18) | copy-start | bytes 4718596
  339.7 8.7 %copy-start.3 = (bf16[256,2048]{1,0:T(8,128)(2,1)S(1)}, bf16[256,2048]{1,0:T(8,128)(2,1)}, u32[]{:S(2)}) copy-start(bf16[256,2048]{1,0:T(8,128)(2,1)} %param.16) | copy-start | bytes 3145732
  339.7 8.7 %copy-start.6 = (bf16[2048,128]{1,0:T(8,128)(2,1)S(1)}, bf16[2048,128]{1,0:T(8,128)(2,1)}, u32[]{:S(2)}) copy-start(bf16[2048,128]{1,0:T(8,128)(2,1)} %param.22) | copy-start | bytes 1572868
  339.7 8.7 %copy-start.11 = (f32[256]{0:T(256)S(1)}, f32[256]{0:T(256)}, u32[]{:S(2)}) copy-start(f32[256]{0:T(256)} %param.29) | copy-start | bytes 3076
  339.7 8.7 %copy-start.12 = (f32[256]{0:T(256)S(1)}, f32[256]{0:T(256)}, u32[]{:S(2)}) copy-start(f32[256]{0:T(256)} %param.28) | copy-start | bytes 3076
  339.7 8.7 %copy-start.14 = (f32[128]{0:T(128)S(1)}, f32[128]{0:T(128)}, u32[]{:S(2)}) copy-start(f32[128]{0:T(128)} %param.23) | copy-start | bytes 1540
  351.1 12.1 %all-to-all-start.3 = ((f32[16,1,512]{2,1,0:T(1,128)}), f32[16,1,512]{2,1,0:T(1,128)S(1)}, u32[]{:S(2)}, u32[]{:S(2)}) async-start(f32[16,1,512]{2,1,0:T(1,128)} %broadcast_in_dim.51), calls=%async_computation.4 | async-start | bytes 65536 | tf_op jit(solution)/shard_map/all_to_all | solution.py:38
  363.2 20.4 %all-to-all-start.2 = ((bf16[16,128,128]{2,1,0:T(8,128)(2,1)}), bf16[16,128,128]{2,1,0:T(8,128)(2,1)S(1)}, u32[]{:S(2)}, u32[]{:S(2)}) async-start(bf16[16,128,128]{2,1,0:T(8,128)(2,1)} %bitcast.17), calls=%async_computation.3 | async-start | bytes 1048576 | tf_op jit(solution)/shard_map/all_to_all | solution.py:32
  370.7 11.0 %collective-permute-start = (f32[128,30]{0,1:T(8,128)S(1)}, f32[128,30]{0,1:T(8,128)S(1)}, u32[]{:S(2)}, u32[]{:S(2)}) collective-permute-start(f32[128,30]{0,1:T(8,128)S(1)} %slice.271), channel_id=1, source_target_pairs={{16,0},{32,16},{48,32},{64,48},{80,64},{96,80},{112,96},{128,112},... | collective-permute-start | bytes 46088 | tf_op jit(solution)/shard_map/ppermute | solution.py:58
  375.8 8.5 %copy-start.1 = (bf16[1,2048,384]{2,1,0:T(8,128)(2,1)S(1)}, bf16[1,2048,384]{2,1,0:T(8,128)(2,1)}, u32[]{:S(2)}) copy-start(bf16[1,2048,384]{2,1,0:T(8,128)(2,1)} %param.19) | copy-start | bytes 4718596
Sparse Core Ops, SparseCore 0:
  177.8 64.3 reduce-scatter.1
  258.0 38.3 all-gather.2
